TPU v7x, 512 devices: a whole 4x4x16 slice. The times are simulated.
512 devices in a mesh: kv: 128 (over z, x, core), tp: 4 (over y).
Axes of the slice: x: 4, y: 4, z: 16, core: 2. Of those that a mesh axis runs over, the one named last changes fastest.
Arguments:
- queries: bfloat16 [16384, 4096], P('kv', 'tp'), may hold values from -6 to 6
- keys: bfloat16 [16384, 512], P('kv', 'tp'), may hold values from -6 to 6
- values: bfloat16 [16384, 512], P('kv', 'tp'), may hold values from -6 to 6
- logsum: float32 [16384, 32], P('kv', 'tp'), may hold values from 2 to 6
- out_grad: bfloat16 [16384, 4096], P('kv', 'tp'), may hold values from -6 to 6
- normed_input: bfloat16 [16384, 4096], P('kv', 'tp'), may hold values from -6 to 6
- chosen: int32 [256, 16], P('kv'), may hold values from 0 to 511, as said below
Outputs:
- query_grad: float32 [16384, 4096], P('kv', 'tp')
- key_grad: float32 [16384, 512], P('kv', 'tp')
- value_grad: float32 [16384, 512], P('kv', 'tp')
- value_weight_grad: float32 [4096, 512], P('kv', 'tp')
Inputs may be any that keep to these rules, and one draw needn't show every extreme that they name: `chosen`: each row r names 16 distinct key blocks, among them block 0 and the blocks r * 2 to r * 2 + 64 / 32 - 1 that hold the query block's own positions. The rows of one device (aligned runs of 2 rows) name at most one block of any other device's 128 / 32 blocks. Blocks after the query block may be named; their keys are masked.
All inputs are finite; a program needn't handle non-finite values.
Results may differ from a plain program's by a relative error of at most 0.008.
Values may be sent and summed in bfloat16 or wider, within the bound.
No kernel may reach another device: no remote copies, remote signals or barrier semaphores. Data moves between devices by JAX's collectives and lax.ppermute only.
A program may use at most 64 MiB of HBM per device.

v0:
```python
import jax
import jax.numpy as jnp
from jax import lax
from jax.sharding import Mesh
from jax.sharding import PartitionSpec as P

HD = 128
QB = 64
KB = 32
NSEL = 16
KV = ("z", "x", "c")
XC = ("x", "c")


def to_peers(parts, axis):
    return lax.all_to_all(parts, axis, split_axis=0, concat_axis=0, tiled=True)


def local(queries, keys, values, logsum, out_grad, normed_input, chosen):
    nz = lax.axis_size("z")
    nq = lax.axis_size(XC)
    tp = lax.axis_size("tp")
    here = lax.axis_index(KV)
    tok = keys.shape[0]
    kblocks = tok // KB
    qblocks = tok // QB
    group = queries.shape[1] // HD
    span = NSEL * KB
    scale = HD ** (-0.5)
    peers = nq * nz
    entries = qblocks * NSEL
    owner = chosen // kblocks
    within = chosen % kblocks
    remote = owner != here
    place = owner % nq * nz + owner // nq
    named = (place[:, :, None] == jnp.arange(peers, dtype=jnp.int32)) & remote[:, :, None]
    wanted = jnp.max(jnp.where(named, within[:, :, None] + 1, 0), axis=(0, 1))
    asked = to_peers(wanted.reshape(nq, nz), XC)
    slot = jnp.where(remote, place, peers + within).reshape(entries)
    taken = jnp.arange(nz, dtype=jnp.int32)[None, :] * kblocks + jnp.maximum(asked - 1, 0)

    def fetch(rows):
        column = lax.all_gather(rows, "z", axis=0, tiled=True).reshape(nz * kblocks, KB, HD)
        got = to_peers(column[taken.reshape(-1)].reshape(nq, nz * KB, HD), XC)
        pool = jnp.concatenate([got.reshape(peers, KB, HD), rows.reshape(kblocks, KB, HD)], axis=0)
        return pool[slot].reshape(qblocks, span, HD)

    onehot = (slot[:, None] == jnp.arange(peers + kblocks, dtype=jnp.int32)[None, :]).astype(
        jnp.float32
    )
    home = ((asked - 1)[:, :, None] == jnp.arange(kblocks, dtype=jnp.int32)).astype(jnp.bfloat16)

    def give_back(part):
        total = jnp.dot(
            onehot.T,
            part.reshape(entries, KB * HD),
            precision=lax.Precision.HIGHEST,
            preferred_element_type=jnp.float32,
        )
        own = total[peers:].reshape(tok, HD)
        sent = total[:peers].astype(jnp.bfloat16).reshape(nq, nz * KB, HD)
        came = to_peers(sent, XC).reshape(nq, nz, KB * HD)
        dense = jnp.einsum("qzk,qze->zke", home, came, preferred_element_type=jnp.float32)
        dense = dense.astype(jnp.bfloat16).reshape(nz, tok, HD)
        sums = to_peers(dense, "z")
        return own + jnp.sum(sums.astype(jnp.float32), axis=0)

    feats = normed_input.shape[1]
    rows_out = feats * tp // peers
    mine = nz // tp
    split = normed_input.reshape(tok, mine, nq, rows_out).transpose(2, 0, 1, 3)
    split = to_peers(split.reshape(nq, tok, mine * rows_out), XC).reshape(nq * tok, mine * rows_out)
    planes = [split]
    for k in range(1, tp):
        planes.append(lax.ppermute(split, "tp", [(i, (i + k) % tp) for i in range(tp)]))
    sel_keys = fetch(keys)
    query_rows = queries.reshape(qblocks, QB, group, HD)
    dout = out_grad.reshape(qblocks, QB, group, HD)
    lse = logsum.reshape(qblocks, QB, group)
    scores = (
        jnp.einsum("bqgd,bjd->bqgj", query_rows, sel_keys, preferred_element_type=jnp.float32)
        * scale
    )
    qpos = here * tok + jnp.arange(tok, dtype=jnp.int32).reshape(qblocks, QB)
    kpos = (chosen[:, :, None] * KB + jnp.arange(KB, dtype=jnp.int32)[None, None, :]).reshape(
        qblocks, span
    )
    valid = (kpos[:, None, :] <= qpos[:, :, None])[:, :, None, :]
    prob = jnp.where(valid, jnp.exp(scores - lse[..., None]), 0.0)
    prob_low = prob.astype(jnp.bfloat16)
    value_grad = give_back(
        jnp.einsum("bqgj,bqgd->bjd", prob_low, dout, preferred_element_type=jnp.float32)
    )
    value_low = value_grad.astype(jnp.bfloat16)
    all_low = lax.all_gather(value_low, XC, axis=0, tiled=True)
    me = lax.axis_index("tp")
    products = jnp.stack(
        [jnp.einsum("tf,tc->fc", p, all_low, preferred_element_type=jnp.float32) for p in planes]
    )
    order = (me - jnp.arange(tp)) % tp
    products = products[order].astype(jnp.bfloat16)
    weight_parts = to_peers(products.reshape(nz, rows_out, HD), "z")
    weight_grad = jnp.sum(weight_parts.astype(jnp.float32), axis=0)
    sel_values = fetch(values)
    dprob = jnp.einsum("bqgd,bjd->bqgj", dout, sel_values, preferred_element_type=jnp.float32)
    delta = jnp.sum(prob * dprob, axis=-1, keepdims=True)
    dscore = (prob * (dprob - delta)).astype(jnp.bfloat16)
    key_grad = give_back(
        jnp.einsum("bqgj,bqgd->bjd", dscore, query_rows, preferred_element_type=jnp.float32) * scale
    )
    query_grad = (
        jnp.einsum("bqgj,bjd->bqgd", dscore, sel_keys, preferred_element_type=jnp.float32) * scale
    )
    return (query_grad.reshape(tok, group * HD), key_grad, value_grad, weight_grad)


def solution(mesh):
    kv, tp = (mesh.shape["kv"], mesh.shape["tp"])
    split = Mesh(mesh.devices.reshape(kv // 8, 4, 2, tp), ("z", "x", "c", "tp"))
    cut = P(KV, "tp")
    return jax.shard_map(
        local,
        mesh=split,
        in_specs=(cut, cut, cut, cut, cut, cut, P(KV, None)),
        out_specs=(cut, cut, cut, cut),
        check_vma=False,
    )
```

profile of v0, /device:TPU:40, one launch (start us, length us, event | category | flops | bytes accessed | tf_op | source)
XLA Modules:
  0.0 260.3 jit_solution(17794559753755833579)
XLA Ops:
  2.1 4.3 %all-to-all-start = ((s32[8,1,16]{2,1,0:T(1,128)}), s32[8,1,16]{2,1,0:T(1,128)S(1)}, u32[]{:S(2)}, u32[]{:S(2)}) async-start(s32[8,1,16]{2,1,0:T(1,128)} %bitcast.1), calls=%async_computation | async-start | bytes 8192 | tf_op jit(solution)/shard_map/all_to_all | solution.py:16
  6.4 36.4 %all_gather.9 = bf16[2048,128]{1,0:T(8,128)(2,1)S(1)} all-gather(bf16[128,128]{1,0:T(8,128)(2,1)} %param.8), channel_id=1, replica_groups=mesh['z'=16,'x'=4,'c'=2,'tp'=4] {'z'}, dimensions={0}, use_global_device_ids=true | all-gather | bytes 557056 | tf_op jit(solution)/shard_map/all_gather | solution.py:43
  43.7 1.7 gather_fusion
  45.4 5.0 %all-to-all-start.1 = ((bf16[8,512,128]{2,1,0:T(8,128)(2,1)}), bf16[8,512,128]{2,1,0:T(8,128)(2,1)S(1)}, u32[]{:S(2)}, u32[]{:S(2)}) async-start(bf16[8,512,128]{2,1,0:T(8,128)(2,1)} %bitcast.4), calls=%async_computation.1 | async-start | bytes 2097152 | tf_op jit(solution)/shard_map/all_to_all | solution.py:16
  52.4 30.9 %all_gather.10 = bf16[2048,128]{1,0:T(8,128)(2,1)S(1)} all-gather(bf16[128,128]{1,0:T(8,128)(2,1)S(1)} %copy-done.10), channel_id=1, replica_groups=mesh['z'=16,'x'=4,'c'=2,'tp'=4] {'z'}, dimensions={0}, use_global_device_ids=true | all-gather | bytes 557056 | tf_op jit(solution)/shard_map/all_gather | solution.py:43
  83.3 1.7 gather_fusion.2
  84.9 4.8 %all-to-all-start.2 = ((bf16[8,512,128]{2,1,0:T(8,128)(2,1)}), bf16[8,512,128]{2,1,0:T(8,128)(2,1)S(1)}, u32[]{:S(2)}, u32[]{:S(2)}) async-start(bf16[8,512,128]{2,1,0:T(8,128)(2,1)} %bitcast.13), calls=%async_computation.2 | async-start | bytes 2097152 | tf_op jit(solution)/shard_map/all_to_all | solution.py:16
  91.0 1.8 gather_fusion.1
  92.8 12.8 %all-to-all-done.2 = bf16[8,512,128]{2,1,0:T(8,128)(2,1)S(1)} async-done(((bf16[8,512,128]{2,1,0:T(8,128)(2,1)}), bf16[8,512,128]{2,1,0:T(8,128)(2,1)S(1)}, u32[]{:S(2)}, u32[]{:S(2)}) %all-to-all-start.2) | async-done | bytes 1048608 | tf_op jit(solution)/shard_map/all_to_all | solution.py:16
  105.6 4.1 %all-to-all-start.7 = ((bf16[8,128,128]{1,2,0:T(8,128)(2,1)}), bf16[8,128,128]{1,2,0:T(8,128)(2,1)}, u32[]{:S(2)}, u32[]{:S(2)}) async-start(bf16[8,128,128]{1,2,0:T(8,128)(2,1)} %bitcast.27), calls=%async_computation.7 | async-start | bytes 524288 | tf_op jit(solution)/shard_map/all_to_all | solution.py:16
  117.6 4.7 %all-to-all-start.5 = ((bf16[8,512,128]{2,1,0:T(8,128)(2,1)}), bf16[8,512,128]{2,1,0:T(8,128)(2,1)S(1)}, u32[]{:S(2)}, u32[]{:S(2)}) async-start(bf16[8,512,128]{2,1,0:T(8,128)(2,1)} %reshape.289), calls=%async_computation.5 | async-start | bytes 2097152 | tf_op jit(solution)/shard_map/all_to_all | solution.py:16
  122.3 1.8 fusion.2
  126.6 2.2 fusion.14
  130.1 2.4 reshape.284
  132.4 5.8 %all-to-all-done.5 = bf16[8,512,128]{2,1,0:T(8,128)(2,1)S(1)} async-done(((bf16[8,512,128]{2,1,0:T(8,128)(2,1)}), bf16[8,512,128]{2,1,0:T(8,128)(2,1)S(1)}, u32[]{:S(2)}, u32[]{:S(2)}) %all-to-all-start.5) | async-done | bytes 1048608 | tf_op jit(solution)/shard_map/all_to_all | solution.py:16
  138.3 4.2 %all-to-all-start.3 = ((bf16[8,512,128]{2,1,0:T(8,128)(2,1)}), bf16[8,512,128]{2,1,0:T(8,128)(2,1)}, u32[]{:S(2)}, u32[]{:S(2)}) async-start(bf16[8,512,128]{2,1,0:T(8,128)(2,1)} %reshape.284), calls=%async_computation.3 | async-start | bytes 2097152 | tf_op jit(solution)/shard_map/all_to_all | solution.py:16
  143.9 2.5 convolution_convert_fusion
  146.4 1.4 reshape.291
  147.8 10.7 %all-to-all-done.3 = bf16[8,512,128]{2,1,0:T(8,128)(2,1)} async-done(((bf16[8,512,128]{2,1,0:T(8,128)(2,1)}), bf16[8,512,128]{2,1,0:T(8,128)(2,1)}, u32[]{:S(2)}, u32[]{:S(2)}) %all-to-all-start.3) | async-done | bytes 1048608 | tf_op jit(solution)/shard_map/all_to_all | solution.py:16
  158.4 7.7 %all-to-all-start.6 = ((bf16[16,128,128]{2,1,0:T(8,128)(2,1)}), bf16[16,128,128]{2,1,0:T(8,128)(2,1)}, u32[]{:S(2)}, u32[]{:S(2)}) async-start(bf16[16,128,128]{2,1,0:T(8,128)(2,1)} %reshape.291), calls=%async_computation.6 | async-start | bytes 1048576 | tf_op jit(solution)/shard_map/all_to_all | solution.py:16
  166.2 1.5 reshape.285
  167.7 2.1 convolution_convert_fusion.1
  169.8 2.4 reshape.286
  172.2 21.9 %all-to-all-done.6 = bf16[16,128,128]{2,1,0:T(8,128)(2,1)} async-done(((bf16[16,128,128]{2,1,0:T(8,128)(2,1)}), bf16[16,128,128]{2,1,0:T(8,128)(2,1)}, u32[]{:S(2)}, u32[]{:S(2)}) %all-to-all-start.6) | async-done | bytes 524320 | tf_op jit(solution)/shard_map/all_to_all | solution.py:16
  194.1 7.3 %all-to-all-start.4 = ((bf16[16,128,128]{2,1,0:T(8,128)(2,1)}), bf16[16,128,128]{2,1,0:T(8,128)(2,1)S(1)}, u32[]{:S(2)}, u32[]{:S(2)}) async-start(bf16[16,128,128]{2,1,0:T(8,128)(2,1)} %reshape.286), calls=%async_computation.4 | async-start | bytes 1048576 | tf_op jit(solution)/shard_map/all_to_all | solution.py:16
  202.5 2.4 collective-permute-start.2
  204.9 4.5 %collective-permute-start.1 = (bf16[1024,128]{1,0:T(8,128)(2,1)S(1)}, bf16[1024,128]{1,0:T(8,128)(2,1)}, u32[]{:S(2)}, u32[]{:S(2)}) collective-permute-start(bf16[1024,128]{1,0:T(8,128)(2,1)S(1)} %bitcast.110), channel_id=1, source_target_pairs={{0,2},{1,3},{2,0},{3,1},{4,6},{5,7},{6,4},{7,5},{8,10},{9,11},{10,... | collective-permute-start | bytes 786440 | tf_op jit(solution)/shard_map/ppermute | solution.py:75
  209.4 3.8 %collective-permute-start = (bf16[1024,128]{1,0:T(8,128)(2,1)S(1)}, bf16[1024,128]{1,0:T(8,128)(2,1)}, u32[]{:S(2)}, u32[]{:S(2)}) collective-permute-start(bf16[1024,128]{1,0:T(8,128)(2,1)S(1)} %bitcast.111), channel_id=1, source_target_pairs={{0,1},{1,2},{2,3},{3,0},{4,5},{5,6},{6,7},{7,4},{8,9},{9,10},{10,1... | collective-permute-start | bytes 786440 | tf_op jit(solution)/shard_map/ppermute | solution.py:75
  215.0 12.8 %all_gather.11 = bf16[1024,128]{1,0:T(8,128)(2,1)S(1)} all-gather(bf16[128,128]{1,0:T(8,128)(2,1)S(1)} %get-tuple-element.4), channel_id=1, replica_groups=mesh['z'=16,'x'=4,'c'=2,'tp'=4] {'x','c'}, dimensions={0}, use_global_device_ids=true | all-gather | bytes 294912 | tf_op jit(solution)/shard_map/all_gather | solution.py:95
  233.2 12.0 %all-to-all-start.8 = ((bf16[16,32,128]{2,1,0:T(8,128)(2,1)}), bf16[16,32,128]{2,1,0:T(8,128)(2,1)S(1)}, u32[]{:S(2)}, u32[]{:S(2)}) async-start(bf16[16,32,128]{2,1,0:T(8,128)(2,1)} %bitcast.38), calls=%async_computation.8 | async-start | bytes 262144 | tf_op jit(solution)/shard_map/all_to_all | solution.py:16
  245.3 2.0 convolution_multiply_fusion
  248.9 10.7 %all-to-all-done.8 = bf16[16,32,128]{2,1,0:T(8,128)(2,1)S(1)} async-done(((bf16[16,32,128]{2,1,0:T(8,128)(2,1)}), bf16[16,32,128]{2,1,0:T(8,128)(2,1)S(1)}, u32[]{:S(2)}, u32[]{:S(2)}) %all-to-all-start.8) | async-done | bytes 131104 | tf_op jit(solution)/shard_map/all_to_all | solution.py:16
  (99 shorter events, 28.9 us)
Async XLA Ops:
  2.1 40.8 %all-to-all-start = ((s32[8,1,16]{2,1,0:T(1,128)}), s32[8,1,16]{2,1,0:T(1,128)S(1)}, u32[]{:S(2)}, u32[]{:S(2)}) async-start(s32[8,1,16]{2,1,0:T(1,128)} %bitcast.1), calls=%async_computation | async-start | bytes 8192 | tf_op jit(solution)/shard_map/all_to_all | solution.py:16
  43.6 7.4 %copy-start.6 = (bf16[128,1024]{1,0:T(8,128)(2,1)S(1)}, bf16[128,1024]{1,0:T(8,128)(2,1)}, u32[]{:S(2)}) copy-start(bf16[128,1024]{1,0:T(8,128)(2,1)} %param.11) | copy-start | bytes 786436
  43.6 7.4 %copy-start.12 = (f32[128,8]{0,1:T(8,128)S(1)}, f32[128,8]{0,1:T(8,128)}, u32[]{:S(2)}) copy-start(f32[128,8]{0,1:T(8,128)} %param.10) | copy-start | bytes 12292
  43.6 7.5 %copy-start.7 = (bf16[128,1024]{1,0:T(8,128)(2,1)S(1)}, bf16[128,1024]{1,0:T(8,128)(2,1)}, u32[]{:S(2)}) copy-start(bf16[128,1024]{1,0:T(8,128)(2,1)} %param.7) | copy-start | bytes 786436
  45.4 6.1 %copy-start.8 = (bf16[128,1024]{1,0:T(8,128)(2,1)S(1)}, bf16[128,1024]{1,0:T(8,128)(2,1)}, u32[]{:S(2)}) copy-start(bf16[128,1024]{1,0:T(8,128)(2,1)} %param.12) | copy-start | bytes 786436
  45.4 7.0 %copy-start.10 = (bf16[128,128]{1,0:T(8,128)(2,1)S(1)}, bf16[128,128]{1,0:T(8,128)(2,1)}, u32[]{:S(2)}) copy-start(bf16[128,128]{1,0:T(8,128)(2,1)} %param.9) | copy-start | bytes 98308
  45.4 39.6 %all-to-all-start.1 = ((bf16[8,512,128]{2,1,0:T(8,128)(2,1)}), bf16[8,512,128]{2,1,0:T(8,128)(2,1)S(1)}, u32[]{:S(2)}, u32[]{:S(2)}) async-start(bf16[8,512,128]{2,1,0:T(8,128)(2,1)} %bitcast.4), calls=%async_computation.1 | async-start | bytes 2097152 | tf_op jit(solution)/shard_map/all_to_all | solution.py:16
  83.3 6.6 %copy-start.9 = (bf16[128,128]{1,0:T(8,128)(2,1)S(1)}, bf16[128,128]{1,0:T(8,128)(2,1)}, u32[]{:S(2)}) copy-start(bf16[128,128]{1,0:T(8,128)(2,1)} %param.8) | copy-start | bytes 98308
  84.9 20.7 %all-to-all-start.2 = ((bf16[8,512,128]{2,1,0:T(8,128)(2,1)}), bf16[8,512,128]{2,1,0:T(8,128)(2,1)S(1)}, u32[]{:S(2)}, u32[]{:S(2)}) async-start(bf16[8,512,128]{2,1,0:T(8,128)(2,1)} %bitcast.13), calls=%async_computation.2 | async-start | bytes 2097152 | tf_op jit(solution)/shard_map/all_to_all | solution.py:16
  92.8 18.0 %copy-start.4 = (bf16[32,32,128]{2,1,0:T(8,128)(2,1)}, bf16[32,32,128]{2,1,0:T(8,128)(2,1)S(1)}, u32[]{:S(2)}) copy-start(bf16[32,32,128]{2,1,0:T(8,128)(2,1)S(1)} %gather_fusion.1) | copy-start | bytes 786436
  105.6 12.0 %all-to-all-start.7 = ((bf16[8,128,128]{1,2,0:T(8,128)(2,1)}), bf16[8,128,128]{1,2,0:T(8,128)(2,1)}, u32[]{:S(2)}, u32[]{:S(2)}) async-start(bf16[8,128,128]{1,2,0:T(8,128)(2,1)} %bitcast.27), calls=%async_computation.7 | async-start | bytes 524288 | tf_op jit(solution)/shard_map/all_to_all | solution.py:16
  111.7 1.3 copy-start
  111.7 2.0 copy-start.13
  114.8 1.4 copy-start.2
  117.6 20.6 %all-to-all-start.5 = ((bf16[8,512,128]{2,1,0:T(8,128)(2,1)}), bf16[8,512,128]{2,1,0:T(8,128)(2,1)S(1)}, u32[]{:S(2)}, u32[]{:S(2)}) async-start(bf16[8,512,128]{2,1,0:T(8,128)(2,1)} %reshape.289), calls=%async_computation.5 | async-start | bytes 2097152 | tf_op jit(solution)/shard_map/all_to_all | solution.py:16
  124.2 1.0 copy-start.3
  128.8 116.5 %copy-start.1 = (f32[132,4096]{1,0:T(8,128)}, f32[132,4096]{1,0:T(8,128)S(1)}, u32[]{:S(2)}) copy-start(f32[132,4096]{1,0:T(8,128)S(1)} %fusion.14) | copy-start | bytes 6488068
  130.1 12.4 %copy-start.11 = (s32[8,16]{1,0:T(8,128)S(1)}, s32[8,16]{1,0:T(8,128)}, u32[]{:S(2)}) copy-start(s32[8,16]{1,0:T(8,128)} %get-tuple-element.9) | copy-start | bytes 1540
  138.3 20.2 %all-to-all-start.3 = ((bf16[8,512,128]{2,1,0:T(8,128)(2,1)}), bf16[8,512,128]{2,1,0:T(8,128)(2,1)}, u32[]{:S(2)}, u32[]{:S(2)}) async-start(bf16[8,512,128]{2,1,0:T(8,128)(2,1)} %reshape.284), calls=%async_computation.3 | async-start | bytes 2097152 | tf_op jit(solution)/shard_map/all_to_all | solution.py:16
  158.4 35.6 %all-to-all-start.6 = ((bf16[16,128,128]{2,1,0:T(8,128)(2,1)}), bf16[16,128,128]{2,1,0:T(8,128)(2,1)}, u32[]{:S(2)}, u32[]{:S(2)}) async-start(bf16[16,128,128]{2,1,0:T(8,128)(2,1)} %reshape.291), calls=%async_computation.6 | async-start | bytes 1048576 | tf_op jit(solution)/shard_map/all_to_all | solution.py:16
  167.7 45.5 %slice-start.1 = ((f32[132,4096]{1,0:T(8,128)}), f32[4,4096]{1,0:T(4,128)S(1)}, s32[]{:S(2)}) async-start(f32[132,4096]{1,0:T(8,128)} %copy-done.2), calls=%async_computation.10 | async-start | bytes 131072 | tf_op jit(solution)/shard_map/slice | solution.py:60
  194.1 39.2 %all-to-all-start.4 = ((bf16[16,128,128]{2,1,0:T(8,128)(2,1)}), bf16[16,128,128]{2,1,0:T(8,128)(2,1)S(1)}, u32[]{:S(2)}, u32[]{:S(2)}) async-start(bf16[16,128,128]{2,1,0:T(8,128)(2,1)} %reshape.286), calls=%async_computation.4 | async-start | bytes 1048576 | tf_op jit(solution)/shard_map/all_to_all | solution.py:16
  202.5 25.6 %collective-permute-start.2 = (bf16[1024,128]{1,0:T(8,128)(2,1)S(1)}, bf16[1024,128]{1,0:T(8,128)(2,1)}, u32[]{:S(2)}, u32[]{:S(2)}) collective-permute-start(bf16[1024,128]{1,0:T(8,128)(2,1)S(1)} %bitcast.109), channel_id=1, source_target_pairs={{0,3},{1,0},{2,1},{3,2},{4,7},{5,4},{6,5},{7,6},{8,11},{9,8},{10,9... | collective-permute-start | bytes 786440 | tf_op jit(solution)/shard_map/ppermute | solution.py:75
  204.9 24.5 %collective-permute-start.1 = (bf16[1024,128]{1,0:T(8,128)(2,1)S(1)}, bf16[1024,128]{1,0:T(8,128)(2,1)}, u32[]{:S(2)}, u32[]{:S(2)}) collective-permute-start(bf16[1024,128]{1,0:T(8,128)(2,1)S(1)} %bitcast.110), channel_id=1, source_target_pairs={{0,2},{1,3},{2,0},{3,1},{4,6},{5,7},{6,4},{7,5},{8,10},{9,11},{10,... | collective-permute-start | bytes 786440 | tf_op jit(solution)/shard_map/ppermute | solution.py:75
  209.4 21.2 %collective-permute-start = (bf16[1024,128]{1,0:T(8,128)(2,1)S(1)}, bf16[1024,128]{1,0:T(8,128)(2,1)}, u32[]{:S(2)}, u32[]{:S(2)}) collective-permute-start(bf16[1024,128]{1,0:T(8,128)(2,1)S(1)} %bitcast.111), channel_id=1, source_target_pairs={{0,1},{1,2},{2,3},{3,0},{4,5},{5,6},{6,7},{7,4},{8,9},{9,10},{10,1... | collective-permute-start | bytes 786440 | tf_op jit(solution)/shard_map/ppermute | solution.py:75
  214.4 30.9 %copy-start.5 = (bf16[32,32,128]{2,1,0:T(8,128)(2,1)S(1)}, bf16[32,32,128]{2,1,0:T(8,128)(2,1)}, u32[]{:S(2)}) copy-start(bf16[32,32,128]{2,1,0:T(8,128)(2,1)} %copy-done.4) | copy-start | bytes 786436
  233.2 26.4 %all-to-all-start.8 = ((bf16[16,32,128]{2,1,0:T(8,128)(2,1)}), bf16[16,32,128]{2,1,0:T(8,128)(2,1)S(1)}, u32[]{:S(2)}, u32[]{:S(2)}) async-start(bf16[16,32,128]{2,1,0:T(8,128)(2,1)} %bitcast.38), calls=%async_computation.8 | async-start | bytes 262144 | tf_op jit(solution)/shard_map/all_to_all | solution.py:16
  245.3 2.9 %slice-start = ((f32[132,4096]{1,0:T(8,128)}), f32[4,4096]{1,0:T(4,128)S(1)}, s32[]{:S(2)}) async-start(f32[132,4096]{1,0:T(8,128)} %copy-done.1), calls=%async_computation.9 | async-start | bytes 131072 | tf_op jit(solution)/shard_map/slice | solution.py:60
where the time goes:
time: 262 us; the launch traced here: 260 us
  blocking collectives  80.2 us (31%)
  starting transfers between devices  64.8 us (25%)
  waiting for transfers between devices  61.9 us (24%)
  local copies, waits for them, and re-layouts  28.5 us (11%)
  matrix products  16.1 us (6%)
  other arithmetic  7.73 us (3%)
    all_gather x2, blocking collectives, fetch(): lax.all_gather(rows, 'z', axis=0, tiled=True).reshape(nz * kblocks, KB, HD)  67.3 us
    all_to_all x9, waiting for transfers between devices, to_peers(): return lax.all_to_all(parts, axis, split_axis=0, concat_axis=0, tiled=True)  61.9 us
    all_to_all x9, starting transfers between devices, to_peers(): return lax.all_to_all(parts, axis, split_axis=0, concat_axis=0, tiled=True)  54.1 us
    all_gather x1, blocking collectives, local(): all_low = lax.all_gather(value_low, XC, axis=0, tiled=True)  12.8 us
    ppermute x3, starting transfers between devices, local(): lax.ppermute(split, 'tp', [(i, (i + k) % tp) for i in range(tp)])  10.7 us
  transfers between devices with their start and end apart: 12, of which 5 were waited for; matrix products, arithmetic and copies ran while one was open for 17% of the time, Pallas kernels for 0%

commit v1 on v0

--- a/solution.py
+++ b/solution.py
@@ -92,7 +92,8 @@
         jnp.einsum("bqgj,bqgd->bjd", prob_low, dout, preferred_element_type=jnp.float32)
     )
     value_low = value_grad.astype(jnp.bfloat16)
-    all_low = lax.all_gather(value_low, XC, axis=0, tiled=True)
+    outgoing = jnp.stack([value_low] * lax.axis_size(XC))
+    all_low = jnp.concatenate(lax.all_to_all(outgoing, XC, 0, 0), axis=0)
     me = lax.axis_index("tp")
     products = jnp.stack(
         [jnp.einsum("tf,tc->fc", p, all_low, preferred_element_type=jnp.float32) for p in planes]

time: 262 us -> 271 us (1.034)
  the two profiles are of different devices: /device:TPU:40 before, /device:TPU:32 now
where the time goes in v1:
time: 271 us; the launch traced here: 270 us
  waiting for transfers between devices  83.6 us (31%)
  blocking collectives  67.4 us (25%)
  starting transfers between devices  64.4 us (24%)
  local copies, waits for them, and re-layouts  28.5 us (11%)
  matrix products  17 us (6%)
  other arithmetic  7.71 us (3%)
    all_to_all x9, waiting for transfers between devices, to_peers(): return lax.all_to_all(parts, axis, split_axis=0, concat_axis=0, tiled=True)  72.8 us
    all_gather x2, blocking collectives, fetch(): lax.all_gather(rows, 'z', axis=0, tiled=True).reshape(nz * kblocks, KB, HD)  67.4 us
    all_to_all x9, starting transfers between devices, to_peers(): return lax.all_to_all(parts, axis, split_axis=0, concat_axis=0, tiled=True)  50.3 us
    ppermute x3, starting transfers between devices, local(): lax.ppermute(split, 'tp', [(i, (i + k) % tp) for i in range(tp)])  10.5 us
    ppermute x3, waiting for transfers between devices, local(): lax.ppermute(split, 'tp', [(i, (i + k) % tp) for i in range(tp)])  8.08 us
  transfers between devices with their start and end apart: 13, of which 11 were waited for; matrix products, arithmetic and copies ran while one was open for 15% of the time, Pallas kernels for 0%

profile of v1, /device:TPU:32, one launch (start us, length us, event | category | flops | bytes accessed | tf_op | source)
XLA Modules:
  0.0 269.7 jit_solution(10144061014065642791)
XLA Ops:
  2.1 4.3 %all-to-all-start = ((s32[8,1,16]{2,1,0:T(1,128)}), s32[8,1,16]{2,1,0:T(1,128)S(1)}, u32[]{:S(2)}, u32[]{:S(2)}) async-start(s32[8,1,16]{2,1,0:T(1,128)} %bitcast.1), calls=%async_computation | async-start | bytes 8192 | tf_op jit(solution)/shard_map/all_to_all | solution.py:16
  6.4 36.4 %all_gather.6 = bf16[2048,128]{1,0:T(8,128)(2,1)S(1)} all-gather(bf16[128,128]{1,0:T(8,128)(2,1)} %param.8), channel_id=1, replica_groups=mesh['z'=16,'x'=4,'c'=2,'tp'=4] {'z'}, dimensions={0}, use_global_device_ids=true | all-gather | bytes 557056 | tf_op jit(solution)/shard_map/all_gather | solution.py:43
  45.3 5.0 %all-to-all-start.1 = ((bf16[8,512,128]{2,1,0:T(8,128)(2,1)}), bf16[8,512,128]{2,1,0:T(8,128)(2,1)S(1)}, u32[]{:S(2)}, u32[]{:S(2)}) async-start(bf16[8,512,128]{2,1,0:T(8,128)(2,1)} %bitcast.4), calls=%async_computation.1 | async-start | bytes 2097152 | tf_op jit(solution)/shard_map/all_to_all | solution.py:16
  51.4 30.9 %all_gather.7 = bf16[2048,128]{1,0:T(8,128)(2,1)S(1)} all-gather(bf16[128,128]{1,0:T(8,128)(2,1)S(1)} %copy-done.10), channel_id=1, replica_groups=mesh['z'=16,'x'=4,'c'=2,'tp'=4] {'z'}, dimensions={0}, use_global_device_ids=true | all-gather | bytes 557056 | tf_op jit(solution)/shard_map/all_gather | solution.py:43
  84.0 4.7 %all-to-all-start.2 = ((bf16[8,512,128]{2,1,0:T(8,128)(2,1)}), bf16[8,512,128]{2,1,0:T(8,128)(2,1)S(1)}, u32[]{:S(2)}, u32[]{:S(2)}) async-start(bf16[8,512,128]{2,1,0:T(8,128)(2,1)} %bitcast.13), calls=%async_computation.2 | async-start | bytes 2097152 | tf_op jit(solution)/shard_map/all_to_all | solution.py:16
  91.9 12.8 %all-to-all-done.2 = bf16[8,512,128]{2,1,0:T(8,128)(2,1)S(1)} async-done(((bf16[8,512,128]{2,1,0:T(8,128)(2,1)}), bf16[8,512,128]{2,1,0:T(8,128)(2,1)S(1)}, u32[]{:S(2)}, u32[]{:S(2)}) %all-to-all-start.2) | async-done | bytes 1048608 | tf_op jit(solution)/shard_map/all_to_all | solution.py:16
  112.7 3.6 %all-to-all-start.5 = ((bf16[8,512,128]{2,1,0:T(8,128)(2,1)}), bf16[8,512,128]{2,1,0:T(8,128)(2,1)S(1)}, u32[]{:S(2)}, u32[]{:S(2)}) async-start(bf16[8,512,128]{2,1,0:T(8,128)(2,1)} %reshape.296), calls=%async_computation.5 | async-start | bytes 2097152 | tf_op jit(solution)/shard_map/all_to_all | solution.py:16
  116.2 1.8 fusion.2
  120.5 2.2 fusion.14
  124.0 2.3 reshape.291
  126.4 5.7 %all-to-all-done.5 = bf16[8,512,128]{2,1,0:T(8,128)(2,1)S(1)} async-done(((bf16[8,512,128]{2,1,0:T(8,128)(2,1)}), bf16[8,512,128]{2,1,0:T(8,128)(2,1)S(1)}, u32[]{:S(2)}, u32[]{:S(2)}) %all-to-all-start.5) | async-done | bytes 1048608 | tf_op jit(solution)/shard_map/all_to_all | solution.py:16
  132.1 4.3 %all-to-all-start.3 = ((bf16[8,512,128]{2,1,0:T(8,128)(2,1)}), bf16[8,512,128]{2,1,0:T(8,128)(2,1)}, u32[]{:S(2)}, u32[]{:S(2)}) async-start(bf16[8,512,128]{2,1,0:T(8,128)(2,1)} %reshape.291), calls=%async_computation.3 | async-start | bytes 2097152 | tf_op jit(solution)/shard_map/all_to_all | solution.py:16
  137.7 2.6 convolution_convert_fusion
  141.6 10.7 %all-to-all-done.3 = bf16[8,512,128]{2,1,0:T(8,128)(2,1)} async-done(((bf16[8,512,128]{2,1,0:T(8,128)(2,1)}), bf16[8,512,128]{2,1,0:T(8,128)(2,1)}, u32[]{:S(2)}, u32[]{:S(2)}) %all-to-all-start.3) | async-done | bytes 1048608 | tf_op jit(solution)/shard_map/all_to_all | solution.py:16
  152.3 7.7 %all-to-all-start.6 = ((bf16[16,128,128]{2,1,0:T(8,128)(2,1)}), bf16[16,128,128]{2,1,0:T(8,128)(2,1)}, u32[]{:S(2)}, u32[]{:S(2)}) async-start(bf16[16,128,128]{2,1,0:T(8,128)(2,1)} %reshape.298), calls=%async_computation.6 | async-start | bytes 1048576 | tf_op jit(solution)/shard_map/all_to_all | solution.py:16
  162.6 25.3 %all-to-all-done.6 = bf16[16,128,128]{2,1,0:T(8,128)(2,1)} async-done(((bf16[16,128,128]{2,1,0:T(8,128)(2,1)}), bf16[16,128,128]{2,1,0:T(8,128)(2,1)}, u32[]{:S(2)}, u32[]{:S(2)}) %all-to-all-start.6) | async-done | bytes 524320 | tf_op jit(solution)/shard_map/all_to_all | solution.py:16
  187.9 4.1 %all-to-all-start.8 = ((bf16[8,128,128]{2,1,0:T(8,128)(2,1)}), bf16[8,128,128]{2,1,0:T(8,128)(2,1)}, u32[]{:S(2)}, u32[]{:S(2)}) async-start(bf16[8,128,128]{2,1,0:T(8,128)(2,1)} %copy.66), calls=%async_computation.8 | async-start | bytes 524288 | tf_op jit(solution)/shard_map/all_to_all | solution.py:16
  193.8 5.6 %all-to-all-done.8 = bf16[8,128,128]{2,1,0:T(8,128)(2,1)} async-done(((bf16[8,128,128]{2,1,0:T(8,128)(2,1)}), bf16[8,128,128]{2,1,0:T(8,128)(2,1)}, u32[]{:S(2)}, u32[]{:S(2)}) %all-to-all-start.8) | async-done | bytes 262176 | tf_op jit(solution)/shard_map/all_to_all | solution.py:16
  200.2 3.6 %all-to-all-start.7 = ((bf16[8,128,128]{1,2,0:T(8,128)(2,1)}), bf16[8,128,128]{1,2,0:T(8,128)(2,1)S(1)}, u32[]{:S(2)}, u32[]{:S(2)}) async-start(bf16[8,128,128]{1,2,0:T(8,128)(2,1)} %stack.12), calls=%async_computation.7 | async-start | bytes 524288 | tf_op jit(solution)/shard_map/all_to_all | solution.py:96
  203.8 2.1 convolution_convert_fusion.1
  205.9 2.4 reshape.293
  208.3 2.8 %all-to-all-done.7 = bf16[8,128,128]{1,2,0:T(8,128)(2,1)S(1)} async-done(((bf16[8,128,128]{1,2,0:T(8,128)(2,1)}), bf16[8,128,128]{1,2,0:T(8,128)(2,1)S(1)}, u32[]{:S(2)}, u32[]{:S(2)}) %all-to-all-start.7) | async-done | bytes 262176 | tf_op jit(solution)/shard_map/all_to_all | solution.py:96
  211.1 7.3 %all-to-all-start.4 = ((bf16[16,128,128]{2,1,0:T(8,128)(2,1)}), bf16[16,128,128]{2,1,0:T(8,128)(2,1)S(1)}, u32[]{:S(2)}, u32[]{:S(2)}) async-start(bf16[16,128,128]{2,1,0:T(8,128)(2,1)} %reshape.293), calls=%async_computation.4 | async-start | bytes 1048576 | tf_op jit(solution)/shard_map/all_to_all | solution.py:16
  218.4 5.1 %collective-permute-start.2 = (bf16[1024,128]{1,0:T(8,128)(2,1)}, bf16[1024,128]{1,0:T(8,128)(2,1)}, u32[]{:S(2)}, u32[]{:S(2)}) collective-permute-start(bf16[1024,128]{1,0:T(8,128)(2,1)} %bitcast.32), channel_id=1, source_target_pairs={{0,3},{1,0},{2,1},{3,2},{4,7},{5,4},{6,5},{7,6},{8,11},{9,8},{10,9... | collective-permute-start | bytes 786440 | tf_op jit(solution)/shard_map/ppermute | solution.py:75
  223.4 2.5 collective-permute-start.1
  226.0 2.9 %collective-permute-start = (bf16[1024,128]{1,0:T(8,128)(2,1)}, bf16[1024,128]{1,0:T(8,128)(2,1)}, u32[]{:S(2)}, u32[]{:S(2)}) collective-permute-start(bf16[1024,128]{1,0:T(8,128)(2,1)} %bitcast.32), channel_id=1, source_target_pairs={{0,1},{1,2},{2,3},{3,0},{4,5},{5,6},{6,7},{7,4},{8,9},{9,10},{10,1... | collective-permute-start | bytes 786440 | tf_op jit(solution)/shard_map/ppermute | solution.py:75
  229.1 4.9 %collective-permute-done.2 = bf16[1024,128]{1,0:T(8,128)(2,1)} collective-permute-done((bf16[1024,128]{1,0:T(8,128)(2,1)}, bf16[1024,128]{1,0:T(8,128)(2,1)}, u32[]{:S(2)}, u32[]{:S(2)}) %collective-permute-start.2) | collective-permute-done | bytes 262176 | tf_op jit(solution)/shard_map/ppermute | solution.py:75
  237.6 2.1 collective-permute-done
  243.4 2.6 all-to-all-done.4
  246.0 9.4 %all-to-all-start.9 = ((bf16[16,32,128]{2,1,0:T(8,128)(2,1)}), bf16[16,32,128]{2,1,0:T(8,128)(2,1)S(1)}, u32[]{:S(2)}, u32[]{:S(2)}) async-start(bf16[16,32,128]{2,1,0:T(8,128)(2,1)} %bitcast.40), calls=%async_computation.9 | async-start | bytes 262144 | tf_op jit(solution)/shard_map/all_to_all | solution.py:16
  255.4 1.9 convolution_multiply_fusion
  259.1 10.0 %all-to-all-done.9 = bf16[16,32,128]{2,1,0:T(8,128)(2,1)S(1)} async-done(((bf16[16,32,128]{2,1,0:T(8,128)(2,1)}), bf16[16,32,128]{2,1,0:T(8,128)(2,1)S(1)}, u32[]{:S(2)}, u32[]{:S(2)}) %all-to-all-start.9) | async-done | bytes 131104 | tf_op jit(solution)/shard_map/all_to_all | solution.py:16
  (103 shorter events, 39.0 us)
Async XLA Ops:
  2.1 40.8 %all-to-all-start = ((s32[8,1,16]{2,1,0:T(1,128)}), s32[8,1,16]{2,1,0:T(1,128)S(1)}, u32[]{:S(2)}, u32[]{:S(2)}) async-start(s32[8,1,16]{2,1,0:T(1,128)} %bitcast.1), calls=%async_computation | async-start | bytes 8192 | tf_op jit(solution)/shard_map/all_to_all | solution.py:16
  43.6 7.4 %copy-start.6 = (bf16[128,1024]{1,0:T(8,128)(2,1)S(1)}, bf16[128,1024]{1,0:T(8,128)(2,1)}, u32[]{:S(2)}) copy-start(bf16[128,1024]{1,0:T(8,128)(2,1)} %param.11) | copy-start | bytes 786436
  43.6 7.4 %copy-start.12 = (f32[128,8]{0,1:T(8,128)S(1)}, f32[128,8]{0,1:T(8,128)}, u32[]{:S(2)}) copy-start(f32[128,8]{0,1:T(8,128)} %param.10) | copy-start | bytes 12292
  43.6 7.5 %copy-start.7 = (bf16[128,1024]{1,0:T(8,128)(2,1)S(1)}, bf16[128,1024]{1,0:T(8,128)(2,1)}, u32[]{:S(2)}) copy-start(bf16[128,1024]{1,0:T(8,128)(2,1)} %param.7) | copy-start | bytes 786436
  45.3 6.1 %copy-start.10 = (bf16[128,128]{1,0:T(8,128)(2,1)S(1)}, bf16[128,128]{1,0:T(8,128)(2,1)}, u32[]{:S(2)}) copy-start(bf16[128,128]{1,0:T(8,128)(2,1)} %param.9) | copy-start | bytes 98308
  45.3 38.7 %all-to-all-start.1 = ((bf16[8,512,128]{2,1,0:T(8,128)(2,1)}), bf16[8,512,128]{2,1,0:T(8,128)(2,1)S(1)}, u32[]{:S(2)}, u32[]{:S(2)}) async-start(bf16[8,512,128]{2,1,0:T(8,128)(2,1)} %bitcast.4), calls=%async_computation.1 | async-start | bytes 2097152 | tf_op jit(solution)/shard_map/all_to_all | solution.py:16
  82.4 6.5 %copy-start.9 = (bf16[128,128]{1,0:T(8,128)(2,1)S(1)}, bf16[128,128]{1,0:T(8,128)(2,1)}, u32[]{:S(2)}) copy-start(bf16[128,128]{1,0:T(8,128)(2,1)} %param.8) | copy-start | bytes 98308
  84.0 20.7 %all-to-all-start.2 = ((bf16[8,512,128]{2,1,0:T(8,128)(2,1)}), bf16[8,512,128]{2,1,0:T(8,128)(2,1)S(1)}, u32[]{:S(2)}, u32[]{:S(2)}) async-start(bf16[8,512,128]{2,1,0:T(8,128)(2,1)} %bitcast.13), calls=%async_computation.2 | async-start | bytes 2097152 | tf_op jit(solution)/shard_map/all_to_all | solution.py:16
  91.9 14.0 %copy-start.4 = (bf16[32,32,128]{2,1,0:T(8,128)(2,1)}, bf16[32,32,128]{2,1,0:T(8,128)(2,1)S(1)}, u32[]{:S(2)}) copy-start(bf16[32,32,128]{2,1,0:T(8,128)(2,1)S(1)} %gather_fusion.1) | copy-start | bytes 786436
  106.7 1.4 copy-start
  106.7 2.0 copy-start.13
  109.9 1.4 copy-start.2
  112.7 19.4 %all-to-all-start.5 = ((bf16[8,512,128]{2,1,0:T(8,128)(2,1)}), bf16[8,512,128]{2,1,0:T(8,128)(2,1)S(1)}, u32[]{:S(2)}, u32[]{:S(2)}) async-start(bf16[8,512,128]{2,1,0:T(8,128)(2,1)} %reshape.296), calls=%async_computation.5 | async-start | bytes 2097152 | tf_op jit(solution)/shard_map/all_to_all | solution.py:16
  118.1 1.0 copy-start.3
  122.7 132.7 %copy-start.1 = (f32[132,4096]{1,0:T(8,128)}, f32[132,4096]{1,0:T(8,128)S(1)}, u32[]{:S(2)}) copy-start(f32[132,4096]{1,0:T(8,128)S(1)} %fusion.14) | copy-start | bytes 6488068
  124.0 12.3 %copy-start.11 = (s32[8,16]{1,0:T(8,128)S(1)}, s32[8,16]{1,0:T(8,128)}, u32[]{:S(2)}) copy-start(s32[8,16]{1,0:T(8,128)} %get-tuple-element.9) | copy-start | bytes 1540
  132.1 20.2 %all-to-all-start.3 = ((bf16[8,512,128]{2,1,0:T(8,128)(2,1)}), bf16[8,512,128]{2,1,0:T(8,128)(2,1)}, u32[]{:S(2)}, u32[]{:S(2)}) async-start(bf16[8,512,128]{2,1,0:T(8,128)(2,1)} %reshape.291), calls=%async_computation.3 | async-start | bytes 2097152 | tf_op jit(solution)/shard_map/all_to_all | solution.py:16
  137.7 22.3 %copy-start.8 = (bf16[128,1024]{1,0:T(8,128)(2,1)S(1)}, bf16[128,1024]{1,0:T(8,128)(2,1)}, u32[]{:S(2)}) copy-start(bf16[128,1024]{1,0:T(8,128)(2,1)} %param.12) | copy-start | bytes 786436
  140.3 20.8 %slice-start.1 = ((f32[132,4096]{1,0:T(8,128)}), f32[4,4096]{1,0:T(4,128)S(1)}, s32[]{:S(2)}) async-start(f32[132,4096]{1,0:T(8,128)} %copy-done.2), calls=%async_computation.11 | async-start | bytes 131072 | tf_op jit(solution)/shard_map/slice | solution.py:60
  152.3 35.6 %all-to-all-start.6 = ((bf16[16,128,128]{2,1,0:T(8,128)(2,1)}), bf16[16,128,128]{2,1,0:T(8,128)(2,1)}, u32[]{:S(2)}, u32[]{:S(2)}) async-start(bf16[16,128,128]{2,1,0:T(8,128)(2,1)} %reshape.298), calls=%async_computation.6 | async-start | bytes 1048576 | tf_op jit(solution)/shard_map/all_to_all | solution.py:16
  187.9 11.6 %all-to-all-start.8 = ((bf16[8,128,128]{2,1,0:T(8,128)(2,1)}), bf16[8,128,128]{2,1,0:T(8,128)(2,1)}, u32[]{:S(2)}, u32[]{:S(2)}) async-start(bf16[8,128,128]{2,1,0:T(8,128)(2,1)} %copy.66), calls=%async_computation.8 | async-start | bytes 524288 | tf_op jit(solution)/shard_map/all_to_all | solution.py:16
  200.2 10.8 %all-to-all-start.7 = ((bf16[8,128,128]{1,2,0:T(8,128)(2,1)}), bf16[8,128,128]{1,2,0:T(8,128)(2,1)S(1)}, u32[]{:S(2)}, u32[]{:S(2)}) async-start(bf16[8,128,128]{1,2,0:T(8,128)(2,1)} %stack.12), calls=%async_computation.7 | async-start | bytes 524288 | tf_op jit(solution)/shard_map/all_to_all | solution.py:96
  211.1 34.9 %all-to-all-start.4 = ((bf16[16,128,128]{2,1,0:T(8,128)(2,1)}), bf16[16,128,128]{2,1,0:T(8,128)(2,1)S(1)}, u32[]{:S(2)}, u32[]{:S(2)}) async-start(bf16[16,128,128]{2,1,0:T(8,128)(2,1)} %reshape.293), calls=%async_computation.4 | async-start | bytes 1048576 | tf_op jit(solution)/shard_map/all_to_all | solution.py:16
  218.4 37.1 %copy-start.5 = (bf16[32,32,128]{2,1,0:T(8,128)(2,1)S(1)}, bf16[32,32,128]{2,1,0:T(8,128)(2,1)}, u32[]{:S(2)}) copy-start(bf16[32,32,128]{2,1,0:T(8,128)(2,1)} %copy-done.4) | copy-start | bytes 786436
  218.4 15.6 %collective-permute-start.2 = (bf16[1024,128]{1,0:T(8,128)(2,1)}, bf16[1024,128]{1,0:T(8,128)(2,1)}, u32[]{:S(2)}, u32[]{:S(2)}) collective-permute-start(bf16[1024,128]{1,0:T(8,128)(2,1)} %bitcast.32), channel_id=1, source_target_pairs={{0,3},{1,0},{2,1},{3,2},{4,7},{5,4},{6,5},{7,6},{8,11},{9,8},{10,9... | collective-permute-start | bytes 786440 | tf_op jit(solution)/shard_map/ppermute | solution.py:75
  223.4 12.9 %collective-permute-start.1 = (bf16[1024,128]{1,0:T(8,128)(2,1)}, bf16[1024,128]{1,0:T(8,128)(2,1)}, u32[]{:S(2)}, u32[]{:S(2)}) collective-permute-start(bf16[1024,128]{1,0:T(8,128)(2,1)} %bitcast.32), channel_id=1, source_target_pairs={{0,2},{1,3},{2,0},{3,1},{4,6},{5,7},{6,4},{7,5},{8,10},{9,11},{10,... | collective-permute-start | bytes 786440 | tf_op jit(solution)/shard_map/ppermute | solution.py:75
  226.0 13.6 %collective-permute-start = (bf16[1024,128]{1,0:T(8,128)(2,1)}, bf16[1024,128]{1,0:T(8,128)(2,1)}, u32[]{:S(2)}, u32[]{:S(2)}) collective-permute-start(bf16[1024,128]{1,0:T(8,128)(2,1)} %bitcast.32), channel_id=1, source_target_pairs={{0,1},{1,2},{2,3},{3,0},{4,5},{5,6},{6,7},{7,4},{8,9},{9,10},{10,1... | collective-permute-start | bytes 786440 | tf_op jit(solution)/shard_map/ppermute | solution.py:75
  246.0 23.1 %all-to-all-start.9 = ((bf16[16,32,128]{2,1,0:T(8,128)(2,1)}), bf16[16,32,128]{2,1,0:T(8,128)(2,1)S(1)}, u32[]{:S(2)}, u32[]{:S(2)}) async-start(bf16[16,32,128]{2,1,0:T(8,128)(2,1)} %bitcast.40), calls=%async_computation.9 | async-start | bytes 262144 | tf_op jit(solution)/shard_map/all_to_all | solution.py:16
  255.4 2.9 %slice-start = ((f32[132,4096]{1,0:T(8,128)}), f32[4,4096]{1,0:T(4,128)S(1)}, s32[]{:S(2)}) async-start(f32[132,4096]{1,0:T(8,128)} %copy-done.1), calls=%async_computation.10 | async-start | bytes 131072 | tf_op jit(solution)/shard_map/slice | solution.py:60
